TPU v7x, 32 devices: a whole 2x2x4 slice. The times are simulated.
32 devices in a mesh: sp: 4 (over z), fs: 4 (over y, x), tp: 2 (over core).
Axes of the slice: x: 2, y: 2, z: 4, core: 2. Of those that a mesh axis runs over, the one named last changes fastest.
Arguments:
- inputs: bfloat16 [4, 2048, 2048], P('fs', 'sp', 'tp'), may hold values from -6 to 6
- norm_gain: float32 [2048], replicated, may hold values from 0.1 to 1.9
- query_weight: bfloat16 [2048, 1024], P(('sp', 'fs'), 'tp'), may hold values from -0.125 to 0.125
- key_weight: bfloat16 [2048, 1024], P(('sp', 'fs'), 'tp'), may hold values from -0.125 to 0.125
- value_weight: bfloat16 [2048, 1024], P(('sp', 'fs'), 'tp'), may hold values from -0.125 to 0.125
- query_gain: float32 [64], replicated, may hold values from 0.8 to 7
- key_gain: float32 [64], replicated, may hold values from 0.8 to 7
- mix_lambda: float32 [8], replicated, may hold values from 0.3 to 0.8
- head_gain: float32 [128], replicated, may hold values from 0.1 to 1.9
- post_gate_weight: bfloat16 [2048, 2048], P(('sp', 'fs'), 'tp'), may hold values from -0.125 to 0.125
- pre_gate_weight: bfloat16 [2048, 2048], P(('sp', 'fs'), 'tp'), may hold values from -0.125 to 0.125
- inner_weight: bfloat16 [2048, 2048], P(('sp', 'fs'), 'tp'), may hold values from -0.125 to 0.125
- conv_taps: float32 [3, 2048], replicated, may hold values from -3 to 3
- attn_out_weight: bfloat16 [2048, 1024], P(('sp', 'fs'), 'tp'), may hold values from -0.109375 to 0.109375
- conv_out_weight: bfloat16 [2048, 2048], P(('sp', 'fs'), 'tp'), may hold values from -0.109375 to 0.109375
Outputs:
- mixed: bfloat16 [4, 2048, 2048], P('fs', ('sp', 'tp'))
All inputs are finite; a program needn't handle non-finite values.
Results may differ from a plain program's by a relative error of at most 0.015.
The roundings to bfloat16 on the way count: a program that leaves them out, or rounds other values in their place, can miss the bound.
Values may be sent and summed in bfloat16 or wider, within the bound.
A program may use at most 128 MiB of HBM per device.

v0:
```python
import math
import jax
import jax.numpy as jnp
from jax import lax
from jax.sharding import PartitionSpec as P

epsilon = 1e-06


def padded_2(x, sides, width):
    for axis, dim in sides:
        size, length = (lax.axis_size(axis), x.shape[dim])
        up = [(i, (i + 1) % size) for i in range(size - 1)]
        down = [(j, i) for i, j in up]
        last = lax.slice_in_dim(x, length - width, length, axis=dim)
        initial = lax.slice_in_dim(x, 0, width, axis=dim)
        before = lax.ppermute(last, axis, up)
        after = lax.ppermute(initial, axis, down)
        x = jnp.concatenate([before, x, after], axis=dim)
    return x


def scale_rows(values, gain):
    return values * lax.rsqrt(jnp.mean(values * values, axis=-1, keepdims=True) + epsilon) * gain


def project_all(normed, weights, products):
    result = []
    for member in range(len(weights)):
        if member < products:
            result.append(jnp.dot(normed, weights[member], preferred_element_type=jnp.float32))
        else:
            result.append(weights[member])
    return tuple(result)


def attention_branch(query, key, values, weight_two, query_gain, key_gain, head_gain):
    tok_rows = query.shape[0]
    vsize = head_gain.shape[0]
    half = query_gain.shape[0]
    heads = values.shape[1] // vsize
    query_normed = scale_rows(query.reshape(tok_rows, heads, 2, half), query_gain).astype(
        jnp.bfloat16
    )
    key_normed = scale_rows(key.reshape(tok_rows, heads * 2, half), key_gain).astype(jnp.bfloat16)
    key_normed = key_normed.reshape(tok_rows, heads * 2 * half)
    scale = half ** (-0.5)
    initial = (
        jnp.full((heads, 2, tok_rows), -1e30, jnp.float32),
        jnp.zeros((heads, 2, tok_rows), jnp.float32),
        jnp.zeros((heads, 2, tok_rows, vsize), jnp.float32),
    )
    carry = initial
    key_piece = lax.all_gather(key_normed, "sp", axis=0, tiled=True)
    value_piece = lax.all_gather(values, "sp", axis=0, tiled=True)
    length = key_piece.shape[0]
    block = math.gcd(length, 512)
    key_blocks = key_piece.reshape(length // block, block, heads, 2, half)
    value_blocks = value_piece.reshape(length // block, block, heads, vsize)

    def one_block(state, blocks):
        peak, total, accum = state
        key_block, value_block = blocks
        scores = (
            jnp.einsum(
                "qhjd,khjd->hjqk", query_normed, key_block, preferred_element_type=jnp.float32
            )
            * scale
        )
        new_peak = jnp.maximum(peak, jnp.max(scores, axis=-1))
        factor = jnp.exp(peak - new_peak)
        expo = jnp.exp(scores - new_peak[..., None])
        total = total * factor + jnp.sum(expo, axis=-1)
        accum = accum * factor[..., None] + jnp.einsum(
            "hjqk,khd->hjqd",
            expo.astype(jnp.bfloat16),
            value_block,
            preferred_element_type=jnp.float32,
        )
        return ((new_peak, total, accum), None)

    carry, unused = lax.scan(one_block, carry, (key_blocks, value_blocks))
    peak, total, accum = carry
    mapped = accum / total[..., None]
    head_out = mapped[:, 0] - weight_two[:, None, None] * mapped[:, 1]
    normed_out = scale_rows(head_out, head_gain).astype(jnp.bfloat16)
    return jnp.transpose(normed_out, (1, 0, 2)).reshape(tok_rows, heads * vsize)


def per_device(
    inputs,
    norm_gain,
    query_weight,
    key_weight,
    value_weight,
    query_gain,
    key_gain,
    mix_lambda,
    head_gain,
    post_gate_weight,
    pre_gate_weight,
    inner_weight,
    conv_taps,
    attn_out_weight,
    conv_out_weight,
):
    tokens = inputs[0]
    whole = lax.all_gather(tokens, "tp", axis=1, tiled=True)
    normed = scale_rows(whole.astype(jnp.float32), norm_gain).astype(jnp.bfloat16)
    heads_dev = value_weight.shape[1] // head_gain.shape[0]
    channels = post_gate_weight.shape[1]
    tp_index = lax.axis_index("tp")
    weight_two = lax.dynamic_slice_in_dim(mix_lambda, tp_index * heads_dev, heads_dev)
    taps = lax.dynamic_slice_in_dim(conv_taps, tp_index * channels, channels, 1)
    every_full = (
        lax.all_gather(query_weight, ("sp", "fs"), axis=0, tiled=True),
        lax.all_gather(key_weight, ("sp", "fs"), axis=0, tiled=True),
        lax.all_gather(value_weight, ("sp", "fs"), axis=0, tiled=True),
        lax.all_gather(post_gate_weight, ("sp", "fs"), axis=0, tiled=True),
        lax.all_gather(pre_gate_weight, ("sp", "fs"), axis=0, tiled=True),
        lax.all_gather(inner_weight, ("sp", "fs"), axis=0, tiled=True),
        lax.all_gather(attn_out_weight, ("sp", "fs"), axis=0, tiled=True),
        lax.all_gather(conv_out_weight, ("sp", "fs"), axis=0, tiled=True),
    )
    query, key, value_proj, post, pre_gate, inner, attn_out_full, conv_out_full = project_all(
        normed, every_full[0:3] + every_full[3:6] + every_full[6:8], 6
    )
    attn_hidden = attention_branch(
        query, key, value_proj.astype(jnp.bfloat16), weight_two, query_gain, key_gain, head_gain
    )
    post_mid = post.astype(jnp.bfloat16)
    post_wide = lax.optimization_barrier(post_mid).astype(jnp.float32)
    signal = (pre_gate * inner).astype(jnp.bfloat16)
    padded = padded_2(signal, (("sp", 0),), 1)
    shifted = lax.optimization_barrier(padded).astype(jnp.float32)
    filtered = taps[0] * shifted[:-2] + taps[1] * shifted[1:-1] + taps[2] * shifted[2:]
    conv_hidden = (post_wide * filtered).astype(jnp.bfloat16)
    contract = (((1,), (1,)), ((), ()))
    summed = lax.psum_scatter(
        (
            lax.dot_general(
                attn_hidden, attn_out_full, contract, preferred_element_type=jnp.float32
            )
            + lax.dot_general(
                conv_hidden, conv_out_full, contract, preferred_element_type=jnp.float32
            )
        ).astype(jnp.bfloat16),
        "tp",
        scatter_dimension=0,
        tiled=True,
    )
    return summed[None]


def solution(mesh):
    placed = (
        P("fs", "sp", "tp"),
        P(),
        P(("sp", "fs"), "tp"),
        P(("sp", "fs"), "tp"),
        P(("sp", "fs"), "tp"),
        P(),
        P(),
        P(),
        P(),
        P(("sp", "fs"), "tp"),
        P(("sp", "fs"), "tp"),
        P(("sp", "fs"), "tp"),
        P(),
        P(("sp", "fs"), "tp"),
        P(("sp", "fs"), "tp"),
    )
    return jax.shard_map(
        per_device,
        mesh=mesh,
        in_specs=placed,
        out_specs=P("fs", ("sp", "tp"), None),
        check_vma=False,
    )
```

profile of v0, /device:TPU:0, one launch (start us, length us, event | category | flops | bytes accessed | tf_op | source)
XLA Modules:
  0.0 693.1 jit_solution(11032667689516088220)
XLA Ops:
  10.1 12.1 %all-gather.33.cloned.1.call-done = bf16[1,512,2048]{2,1,0:T(8,128)(2,1)} async-done(((bf16[1,512,1024]{2,1,0:T(8,128)(2,1)}), bf16[1,512,2048]{2,1,0:T(8,128)(2,1)}) %all-gather.33.cloned.1.call-update) | async-done | bytes 2097168 | tf_op jit(solution)/shard_map/all_gather | solution.py:108
  24.4 62.1 %all-gather.13.cloned.1.call-done = bf16[2048,512]{1,0:T(8,128)(2,1)} async-done(((bf16[128,512]{1,0:T(8,128)(2,1)}), bf16[2048,512]{1,0:T(8,128)(2,1)}) %all-gather.13.cloned.1.call-update) | async-done | bytes 2097168 | tf_op jit(solution)/shard_map/all_gather | solution.py:117
  90.6 57.9 %all-gather.19.cloned.1.call-done = bf16[2048,512]{1,0:T(8,128)(2,1)} async-done(((bf16[128,512]{1,0:T(8,128)(2,1)}), bf16[2048,512]{1,0:T(8,128)(2,1)}) %all-gather.19.cloned.1.call-update) | async-done | bytes 2097168 | tf_op jit(solution)/shard_map/all_gather | solution.py:118
  148.6 3.7 convolution_convert_fusion.1
  157.1 53.3 %all-gather.17.cloned.1.call-done = bf16[2048,512]{1,0:T(8,128)(2,1)} async-done(((bf16[128,512]{1,0:T(8,128)(2,1)}), bf16[2048,512]{1,0:T(8,128)(2,1)}) %all-gather.17.cloned.1.call-update) | async-done | bytes 2097168 | tf_op jit(solution)/shard_map/all_gather | solution.py:116
  210.4 3.6 multiply_reduce_fusion.1
  214.3 42.0 %all-gather.15.cloned.1.call-done = bf16[2048,512]{0,1:T(8,128)(2,1)} async-done(((bf16[512,512]{0,1:T(8,128)(2,1)}), bf16[2048,512]{0,1:T(8,128)(2,1)}) %all-gather.15.cloned.1.call-update) | async-done | bytes 2097168 | tf_op jit(solution)/shard_map/all_gather | solution.py:54
  256.3 4.5 reshape.57
  260.8 3.4 copy.21
  264.2 38.0 %all-gather.21.cloned.1.call-done = bf16[2048,512]{1,0:T(8,128)(2,1)} async-done(((bf16[512,512]{1,0:T(8,128)(2,1)}), bf16[2048,512]{1,0:T(8,128)(2,1)}) %all-gather.21.cloned.1.call-update) | async-done | bytes 2097168 | tf_op jit(solution)/shard_map/all_gather | solution.py:55
  302.2 4.0 reshape.59
  306.2 59.2 %while.15 = (s32[]{:T(128)}, f32[4,2,512]{2,1,0:T(2,128)S(1)}, f32[4,2,512]{2,1,0:T(2,128)S(1)}, f32[4,2,512,128]{3,2,1,0:T(8,128)S(1)}, bf16[4,512,4,2,64]{1,4,...) while((s32[]{:T(128)}, f32[4,2,512]{2,1,0:T(2,128)S(1)}, ...), condition=%wide.region_6.7_spmd.clone, body=%wide.region_3.6_spmd.clone.sunk | while | flops 823676928 | bytes 65798792 | solution.py:82
  306.2 5.6 bitcast_reduce_fusion.3
  311.9 5.1 fusion.62
  321.0 5.6 bitcast_reduce_fusion.3
  326.7 5.0 fusion.62
  335.8 5.6 bitcast_reduce_fusion.3
  341.4 5.0 fusion.62
  350.5 5.8 bitcast_reduce_fusion.3
  356.3 5.0 fusion.62
  370.1 9.3 %all-gather.27.cloned.1.call-done = bf16[2048,1024]{1,0:T(8,128)(2,1)} async-done(((bf16[128,1024]{1,0:T(8,128)(2,1)}), bf16[2048,1024]{1,0:T(8,128)(2,1)}) %all-gather.27.cloned.1.call-update) | async-done | bytes 4194320 | tf_op jit(solution)/shard_map/all_gather | solution.py:120
  379.4 5.9 fusion.34
  385.3 71.1 %all-gather.29.cloned.1.call-done = bf16[2048,1024]{1,0:T(8,128)(2,1)} async-done(((bf16[128,1024]{1,0:T(8,128)(2,1)}), bf16[2048,1024]{1,0:T(8,128)(2,1)}) %all-gather.29.cloned.1.call-update) | async-done | bytes 4194320 | tf_op jit(solution)/shard_map/all_gather | solution.py:121
  456.4 5.2 multiply_convert_fusion
  462.6 3.4 collective-permute-start
  467.5 65.9 %all-gather.25.cloned.1.call-done = bf16[2048,1024]{1,0:T(8,128)(2,1)} async-done(((bf16[128,1024]{1,0:T(8,128)(2,1)}), bf16[2048,1024]{1,0:T(8,128)(2,1)}) %all-gather.25.cloned.1.call-update) | async-done | bytes 4194320 | tf_op jit(solution)/shard_map/all_gather | solution.py:119
  533.4 5.7 convolution_convert_fusion
  539.6 70.6 %all-gather.31.cloned.1.call-done = bf16[2048,1024]{1,0:T(8,128)(2,1)} async-done(((bf16[128,1024]{1,0:T(8,128)(2,1)}), bf16[2048,1024]{1,0:T(8,128)(2,1)}) %all-gather.31.cloned.1.call-update) | async-done | bytes 4194320 | tf_op jit(solution)/shard_map/all_gather | solution.py:123
  610.2 7.1 %fusion.24 = f32[512,2048]{1,0:T(8,128)} fusion(bf16[2048,1024]{1,0:T(8,128)(2,1)} %all-gather.31.cloned.1.call-done, f32[514,1024]{1,0:T(8,128)S(1)} %convert_element_type.49, bf16[512,1024]{1,0:T(8,128)(2,1)} %convolution_convert_fusion, f32[1024]{0:T(1024)S(1)} %bitcast.100, f32[1024]{0:T(1024)S(1)} %bitcast.99, f32[1024]{0:T(1024)S(1)} %bitcast.98), kind=kOutput, calls=%fused_computation.39 | convolution fusion | flops 2151677952 | bytes 15740928 | tf_op jit(solution)/shard_map/dot_general | solution.py:144
  617.4 54.7 %all-gather.23.cloned.1.call-done = bf16[2048,512]{1,0:T(8,128)(2,1)} async-done(((bf16[128,512]{1,0:T(8,128)(2,1)}), bf16[2048,512]{1,0:T(8,128)(2,1)}) %all-gather.23.cloned.1.call-update) | async-done | bytes 2097168 | tf_op jit(solution)/shard_map/all_gather | solution.py:122
  672.0 5.5 add_convert_fusion
  677.6 8.7 %reduce-scatter.2.cloned.1.call-done = bf16[256,2048]{1,0:T(8,128)(2,1)} async-done(((bf16[512,2048]{1,0:T(8,128)(2,1)}), bf16[256,2048]{1,0:T(8,128)(2,1)}) %reduce-scatter.2.cloned.1.call-update) | async-done | bytes 1048592 | tf_op jit(solution)/shard_map/reduce_scatter | solution.py:139
  (94 shorter events, 38.7 us)
Async XLA Ops:
  6.5 80.0 %copy-start.7 = (f32[2048]{0:T(1024)S(1)}, f32[2048]{0:T(1024)}, u32[]{:S(2)}) copy-start(f32[2048]{0:T(1024)} %param.18) | copy-start | bytes 24580
  6.5 15.7 %all-gather.33.cloned.1.call-start = ((), (), s32[]{:S(2)}) async-start(), calls=%async_computation.12 | async-start | bytes 3145728 | tf_op jit(solution)/shard_map/all_gather | solution.py:108
  7.3 79.3 %all-gather.13.cloned.1.call-start = ((), (), s32[]{:S(2)}) async-start(), calls=%async_computation.1 | async-start | bytes 2228224 | tf_op jit(solution)/shard_map/all_gather | solution.py:117
  8.0 140.5 %all-gather.19.cloned.1.call-start = ((), (), s32[]{:S(2)}) async-start(), calls=%async_computation.4 | async-start | bytes 2228224 | tf_op jit(solution)/shard_map/all_gather | solution.py:118
  8.7 201.6 %all-gather.17.cloned.1.call-start = ((), (), s32[]{:S(2)}) async-start(), calls=%async_computation.3 | async-start | bytes 2228224 | tf_op jit(solution)/shard_map/all_gather | solution.py:116
  9.3 247.0 %all-gather.15.cloned.1.call-start = ((), (), s32[]{:S(2)}) async-start(), calls=%async_computation.2 | async-start | bytes 2621440 | tf_op jit(solution)/shard_map/all_gather | solution.py:54
  22.2 64.4 %copy-start.1 = (bf16[1,512,2048]{2,1,0:T(8,128)(2,1)S(1)}, bf16[1,512,2048]{2,1,0:T(8,128)(2,1)}, u32[]{:S(2)}) copy-start(bf16[1,512,2048]{2,1,0:T(8,128)(2,1)} %all-gather.33.cloned.1.call-done) | copy-start | bytes 6291460
  90.6 65.5 %copy-start.8 = (f32[8]{0:T(128)S(1)}, f32[8]{0:T(128)}, u32[]{:S(2)}) copy-start(f32[8]{0:T(128)} %param.24) | copy-start | bytes 100
  90.6 211.6 %all-gather.21.cloned.1.call-start = ((), (), s32[]{:S(2)}) async-start(), calls=%async_computation.5 | async-start | bytes 2621440 | tf_op jit(solution)/shard_map/all_gather | solution.py:55
  152.3 227.1 %all-gather.27.cloned.1.call-start = ((), (), s32[]{:S(2)}) async-start(), calls=%async_computation.8 | async-start | bytes 4456448 | tf_op jit(solution)/shard_map/all_gather | solution.py:120
  153.0 303.4 %all-gather.29.cloned.1.call-start = ((), (), s32[]{:S(2)}) async-start(), calls=%async_computation.9 | async-start | bytes 4456448 | tf_op jit(solution)/shard_map/all_gather | solution.py:121
  153.8 379.6 %all-gather.25.cloned.1.call-start = ((), (), s32[]{:S(2)}) async-start(), calls=%async_computation.7 | async-start | bytes 4456448 | tf_op jit(solution)/shard_map/all_gather | solution.py:119
  154.5 455.7 %all-gather.31.cloned.1.call-start = ((), (), s32[]{:S(2)}) async-start(), calls=%async_computation.10 | async-start | bytes 4456448 | tf_op jit(solution)/shard_map/all_gather | solution.py:123
  155.1 516.9 %all-gather.23.cloned.1.call-start = ((), (), s32[]{:S(2)}) async-start(), calls=%async_computation.6 | async-start | bytes 2228224 | tf_op jit(solution)/shard_map/all_gather | solution.py:122
  155.8 530.4 %reduce-scatter.2.cloned.1.call-start = ((), (), s32[]{:S(2)}) async-start(), calls=%async_computation.11 | async-start | bytes 3145728 | tf_op jit(solution)/shard_map/reduce_scatter | solution.py:139
  157.1 57.0 %copy-start.5 = (f32[64]{0:T(128)S(1)}, f32[64]{0:T(128)}, u32[]{:S(2)}) copy-start(f32[64]{0:T(128)} %param.22) | copy-start | bytes 772
  311.8 6.4 copy-start
  326.7 6.3 copy-start
  341.4 6.3 copy-start
  356.3 6.3 copy-start
  369.2 0.7 copy-start.6
  369.2 10.2 %copy-start.2 = (bf16[1,512,2048]{2,1,0:T(8,128)(2,1)S(1)}, bf16[1,512,2048]{2,1,0:T(8,128)(2,1)}, u32[]{:S(2)}) copy-start(bf16[1,512,2048]{2,1,0:T(8,128)(2,1)} %all-gather.33.cloned.1.call-done) | copy-start | bytes 6291460
  461.6 1.0 copy-start.3
  462.6 76.5 %collective-permute-start = (bf16[1,1024]{1,0:T(2,128)(2,1)S(1)}, bf16[1,1024]{1,0:T(2,128)(2,1)S(1)}, u32[]{:S(2)}, u32[]{:S(2)}) collective-permute-start(bf16[1,1024]{1,0:T(2,128)(2,1)S(1)} %get-tuple-element.101), channel_id=1, source_target_pairs={{0,8},{8,16},{16,24},{1,9},{9,17},{17,25},{2,10},{10,18},{18,26},{... | collective-permute-start | bytes 6152 | tf_op jit(solution)/shard_map/ppermute | solution.py:17
  466.0 73.1 %collective-permute-start.1 = (bf16[1,1024]{1,0:T(2,128)(2,1)S(1)}, bf16[1,1024]{1,0:T(2,128)(2,1)S(1)}, u32[]{:S(2)}, u32[]{:S(2)}) collective-permute-start(bf16[1,1024]{1,0:T(2,128)(2,1)S(1)} %get-tuple-element.102), channel_id=1, source_target_pairs={{8,0},{16,8},{24,16},{9,1},{17,9},{25,17},{10,2},{18,10},{26,18},{... | collective-permute-start | bytes 6152 | tf_op jit(solution)/shard_map/ppermute | solution.py:18
  533.4 5.7 copy-start.4
Sparse Core Ops, SparseCore 0:
  8.9 13.2 all-gather.32
  25.0 61.5 all-gather.12
  89.3 59.1 all-gather.18
  151.2 59.1 all-gather.16
  211.8 44.4 all-gather.14
  257.7 44.4 all-gather.20
  305.0 74.3 all-gather.26
  382.2 74.1 all-gather.28
  459.2 74.1 all-gather.24
  536.0 74.1 all-gather.30
  613.0 58.9 all-gather.22
  677.7 8.5 reduce-scatter.1
where the time goes:
time: 694 us; the launch traced here: 693 us
  waiting for transfers between devices  552 us (80%)
  matrix products  73.6 us (11%)
  other arithmetic  26.6 us (4%)
  local copies, waits for them, and re-layouts  21.7 us (3%)
  between operations  13.8 us (2%)
    all_gather x1, waiting for transfers between devices, per_device(): lax.all_gather(inner_weight, ('sp', 'fs'), axis=0, tiled=True)  71.1 us
    all_gather x1, waiting for transfers between devices, per_device(): lax.all_gather(conv_out_weight, ('sp', 'fs'), axis=0, tiled=True)  70.6 us
    all_gather x1, waiting for transfers between devices, per_device(): lax.all_gather(post_gate_weight, ('sp', 'fs'), axis=0, tiled=True)  65.9 us
    all_gather x1, waiting for transfers between devices, per_device(): lax.all_gather(key_weight, ('sp', 'fs'), axis=0, tiled=True)  62.1 us
    all_gather x1, waiting for transfers between devices, per_device(): lax.all_gather(value_weight, ('sp', 'fs'), axis=0, tiled=True)  57.9 us
    all_gather x1, waiting for transfers between devices, per_device(): lax.all_gather(attn_out_weight, ('sp', 'fs'), axis=0, tiled=True)  54.7 us
    all_gather x1, waiting for transfers between devices, per_device(): lax.all_gather(query_weight, ('sp', 'fs'), axis=0, tiled=True)  53.3 us
    all_gather x1, waiting for transfers between devices, attention_branch(): key_piece = lax.all_gather(key_normed, 'sp', axis=0, tiled=True)  42 us
  transfers between devices with their start and end apart: 14, of which 12 were waited for; matrix products, arithmetic and copies ran while one was open for 17% of the time, Pallas kernels for 0%

commit v1 on v0

--- a/solution.py
+++ b/solution.py
@@ -51,7 +51,12 @@
         jnp.zeros((heads, 2, tok_rows, vsize), jnp.float32),
     )
     carry = initial
-    key_piece = lax.all_gather(key_normed, "sp", axis=0, tiled=True)
+    ring = [key_normed]
+    for hop in range(3):
+        ring.append(lax.ppermute(ring[-1], "sp", [(dev, (dev + 1) % 4) for dev in range(4)]))
+    key_piece = jnp.roll(
+        jnp.concatenate(ring[::-1], axis=0), (lax.axis_index("sp") + 1) * ring[0].shape[0], axis=0
+    )
     value_piece = lax.all_gather(values, "sp", axis=0, tiled=True)
     length = key_piece.shape[0]
     block = math.gcd(length, 512)

time: 694 us -> 658 us (0.948)
  waiting for transfers between devices: 552 us -> 509 us
    all_gather x1 -> x0, waiting for transfers between devices: 42 us -> none  [attention_branch(): key_piece = lax.all_gather(key_normed, 'sp', axis=0, tiled=True)]
    ppermute x0 -> x3, waiting for transfers between devices: none -> 27.2 us  [attention_branch(): lax.ppermute(ring[-1], 'sp', [(dev, (dev + 1) % 4) for dev in range(4)])]
    all_gather x1, waiting for transfers between devices: 53.3 us -> 39 us  [per_device(): lax.all_gather(query_weight, ('sp', 'fs'), axis=0, tiled=True)]
    all_gather x1, waiting for transfers between devices: 38 us -> 27.6 us  [attention_branch(): value_piece = lax.all_gather(values, 'sp', axis=0, tiled=True)]
    all_gather x1, waiting for transfers between devices: 62.1 us -> 54.7 us  [per_device(): lax.all_gather(key_weight, ('sp', 'fs'), axis=0, tiled=True)]
  transfers between devices with their start and end apart: 14 -> 16, of which waited for: 12 -> 13; matrix products, arithmetic and copies ran while one was open for 17% -> 18% of each run, Pallas kernels for 0% -> 0%
where the time goes in v1:
time: 658 us; the launch traced here: 657 us
  waiting for transfers between devices  509 us (77%)
  matrix products  74.3 us (11%)
  local copies, waits for them, and re-layouts  27.2 us (4%)
  other arithmetic  25.7 us (4%)
  between operations  13.6 us (2%)
  starting transfers between devices  6.8 us (1%)
    all_gather x1, waiting for transfers between devices, per_device(): lax.all_gather(inner_weight, ('sp', 'fs'), axis=0, tiled=True)  71.1 us
    all_gather x1, waiting for transfers between devices, per_device(): lax.all_gather(conv_out_weight, ('sp', 'fs'), axis=0, tiled=True)  70.7 us
    all_gather x1, waiting for transfers between devices, per_device(): lax.all_gather(post_gate_weight, ('sp', 'fs'), axis=0, tiled=True)  65.8 us
    all_gather x1, waiting for transfers between devices, per_device(): lax.all_gather(value_weight, ('sp', 'fs'), axis=0, tiled=True)  62.2 us
    all_gather x1, waiting for transfers between devices, per_device(): lax.all_gather(key_weight, ('sp', 'fs'), axis=0, tiled=True)  54.7 us
    all_gather x1, waiting for transfers between devices, per_device(): lax.all_gather(attn_out_weight, ('sp', 'fs'), axis=0, tiled=True)  54.5 us
    all_gather x1, waiting for transfers between devices, per_device(): lax.all_gather(query_weight, ('sp', 'fs'), axis=0, tiled=True)  39 us
    dot_general x6, matrix products, project_all(): jnp.dot(normed, weights[member], preferred_element_type=jnp.float32)  27.8 us
  transfers between devices with their start and end apart: 16, of which 13 were waited for; matrix products, arithmetic and copies ran while one was open for 18% of the time, Pallas kernels for 0%

profile of v1, /device:TPU:0, one launch (start us, length us, event | category | flops | bytes accessed | tf_op | source)
XLA Modules:
  0.0 656.9 jit_solution(4951756206929355065)
XLA Ops:
  9.4 12.8 %all-gather.30.cloned.1.call-done = bf16[1,512,2048]{2,1,0:T(8,128)(2,1)} async-done(((bf16[1,512,1024]{2,1,0:T(8,128)(2,1)}), bf16[1,512,2048]{2,1,0:T(8,128)(2,1)}) %all-gather.30.cloned.1.call-update) | async-done | bytes 2097168 | tf_op jit(solution)/shard_map/all_gather | solution.py:113
  24.3 62.2 %all-gather.16.cloned.1.call-done = bf16[2048,512]{1,0:T(8,128)(2,1)} async-done(((bf16[128,512]{1,0:T(8,128)(2,1)}), bf16[2048,512]{1,0:T(8,128)(2,1)}) %all-gather.16.cloned.1.call-update) | async-done | bytes 2097168 | tf_op jit(solution)/shard_map/all_gather | solution.py:123
  86.6 4.3 convolution_convert_fusion.1
  93.9 54.7 %all-gather.12.cloned.1.call-done = bf16[2048,512]{1,0:T(8,128)(2,1)} async-done(((bf16[128,512]{1,0:T(8,128)(2,1)}), bf16[2048,512]{1,0:T(8,128)(2,1)}) %all-gather.12.cloned.1.call-update) | async-done | bytes 2097168 | tf_op jit(solution)/shard_map/all_gather | solution.py:122
  153.3 15.0 %collective-permute-done = bf16[512,512]{0,1:T(8,128)(2,1)S(1)} collective-permute-done((bf16[512,512]{0,1:T(8,128)(2,1)S(1)}, bf16[512,512]{0,1:T(8,128)(2,1)S(1)}, u32[]{:S(2)}, u32[]{:S(2)}) %collective-permute-start) | collective-permute-done | bytes 524320 | tf_op jit(solution)/shard_map/ppermute | solution.py:56
  169.4 12.2 %collective-permute-done.1 = bf16[512,512]{0,1:T(8,128)(2,1)} collective-permute-done((bf16[512,512]{0,1:T(8,128)(2,1)S(1)}, bf16[512,512]{0,1:T(8,128)(2,1)}, u32[]{:S(2)}, u32[]{:S(2)}) %collective-permute-start.1) | collective-permute-done | bytes 524320 | tf_op jit(solution)/shard_map/ppermute | solution.py:56
  181.6 39.0 %all-gather.14.cloned.1.call-done = bf16[2048,512]{1,0:T(8,128)(2,1)} async-done(((bf16[128,512]{1,0:T(8,128)(2,1)}), bf16[2048,512]{1,0:T(8,128)(2,1)}) %all-gather.14.cloned.1.call-update) | async-done | bytes 2097168 | tf_op jit(solution)/shard_map/all_gather | solution.py:121
  220.6 3.6 multiply_reduce_fusion.1
  231.0 4.5 reshape.57
  235.5 3.4 copy.20
  238.9 27.6 %all-gather.18.cloned.1.call-done = bf16[2048,512]{1,0:T(8,128)(2,1)} async-done(((bf16[512,512]{1,0:T(8,128)(2,1)}), bf16[2048,512]{1,0:T(8,128)(2,1)}) %all-gather.18.cloned.1.call-update) | async-done | bytes 2097168 | tf_op jit(solution)/shard_map/all_gather | solution.py:60
  266.5 4.0 reshape.59
  270.5 59.3 %while.15 = (s32[]{:T(128)}, f32[4,2,512]{2,1,0:T(2,128)S(1)}, f32[4,2,512]{2,1,0:T(2,128)S(1)}, f32[4,2,512,128]{3,2,1,0:T(8,128)S(1)}, bf16[4,512,4,2,64]{1,4,...) while((s32[]{:T(128)}, f32[4,2,512]{2,1,0:T(2,128)S(1)}, ...), condition=%wide.region_6.7_spmd.clone, body=%wide.region_3.6_spmd.clone.sunk | while | flops 823676928 | bytes 65798792 | solution.py:87
  270.5 5.6 bitcast_reduce_fusion.3
  276.2 5.1 fusion.62
  285.3 5.6 bitcast_reduce_fusion.3
  291.0 5.0 fusion.62
  300.1 5.6 bitcast_reduce_fusion.3
  305.7 5.0 fusion.62
  314.8 5.8 bitcast_reduce_fusion.3
  320.7 5.0 fusion.62
  334.1 9.4 %all-gather.24.cloned.1.call-done = bf16[2048,1024]{1,0:T(8,128)(2,1)} async-done(((bf16[128,1024]{1,0:T(8,128)(2,1)}), bf16[2048,1024]{1,0:T(8,128)(2,1)}) %all-gather.24.cloned.1.call-update) | async-done | bytes 4194320 | tf_op jit(solution)/shard_map/all_gather | solution.py:125
  343.5 5.9 fusion.34
  349.5 71.1 %all-gather.26.cloned.1.call-done = bf16[2048,1024]{1,0:T(8,128)(2,1)} async-done(((bf16[128,1024]{1,0:T(8,128)(2,1)}), bf16[2048,1024]{1,0:T(8,128)(2,1)}) %all-gather.26.cloned.1.call-update) | async-done | bytes 4194320 | tf_op jit(solution)/shard_map/all_gather | solution.py:126
  420.5 5.2 multiply_convert_fusion
  431.7 65.8 %all-gather.22.cloned.1.call-done = bf16[2048,1024]{1,0:T(8,128)(2,1)} async-done(((bf16[128,1024]{1,0:T(8,128)(2,1)}), bf16[2048,1024]{1,0:T(8,128)(2,1)}) %all-gather.22.cloned.1.call-update) | async-done | bytes 4194320 | tf_op jit(solution)/shard_map/all_gather | solution.py:124
  497.5 5.7 convolution_convert_fusion
  503.8 70.7 %all-gather.28.cloned.1.call-done = bf16[2048,1024]{1,0:T(8,128)(2,1)} async-done(((bf16[128,1024]{1,0:T(8,128)(2,1)}), bf16[2048,1024]{1,0:T(8,128)(2,1)}) %all-gather.28.cloned.1.call-update) | async-done | bytes 4194320 | tf_op jit(solution)/shard_map/all_gather | solution.py:128
  574.5 7.1 %fusion.24 = f32[512,2048]{1,0:T(8,128)} fusion(bf16[2048,1024]{1,0:T(8,128)(2,1)} %all-gather.28.cloned.1.call-done, f32[514,1024]{1,0:T(8,128)S(1)} %convert_element_type.49, bf16[512,1024]{1,0:T(8,128)(2,1)} %convolution_convert_fusion, f32[1024]{0:T(1024)S(1)} %bitcast.100, f32[1024]{0:T(1024)S(1)} %bitcast.99, f32[1024]{0:T(1024)S(1)} %bitcast.98), kind=kOutput, calls=%fused_computation.39 | convolution fusion | flops 2151677952 | bytes 15740928 | tf_op jit(solution)/shard_map/dot_general | solution.py:149
  581.6 54.5 %all-gather.20.cloned.1.call-done = bf16[2048,512]{1,0:T(8,128)(2,1)} async-done(((bf16[128,512]{1,0:T(8,128)(2,1)}), bf16[2048,512]{1,0:T(8,128)(2,1)}) %all-gather.20.cloned.1.call-update) | async-done | bytes 2097168 | tf_op jit(solution)/shard_map/all_gather | solution.py:127
  636.2 5.5 add_convert_fusion
  641.7 8.7 %reduce-scatter.2.cloned.1.call-done = bf16[256,2048]{1,0:T(8,128)(2,1)} async-done(((bf16[512,2048]{1,0:T(8,128)(2,1)}), bf16[256,2048]{1,0:T(8,128)(2,1)}) %reduce-scatter.2.cloned.1.call-update) | async-done | bytes 1048592 | tf_op jit(solution)/shard_map/reduce_scatter | solution.py:144
  (112 shorter events, 47.3 us)
Async XLA Ops:
  6.5 80.0 %copy-start.10 = (f32[2048]{0:T(1024)S(1)}, f32[2048]{0:T(1024)}, u32[]{:S(2)}) copy-start(f32[2048]{0:T(1024)} %param.18) | copy-start | bytes 24580
  6.5 15.7 %all-gather.30.cloned.1.call-start = ((), (), s32[]{:S(2)}) async-start(), calls=%async_computation.11 | async-start | bytes 3145728 | tf_op jit(solution)/shard_map/all_gather | solution.py:113
  7.3 79.3 %all-gather.16.cloned.1.call-start = ((), (), s32[]{:S(2)}) async-start(), calls=%async_computation.3 | async-start | bytes 2228224 | tf_op jit(solution)/shard_map/all_gather | solution.py:123
  8.0 140.5 %all-gather.12.cloned.1.call-start = ((), (), s32[]{:S(2)}) async-start(), calls=%async_computation.1 | async-start | bytes 2228224 | tf_op jit(solution)/shard_map/all_gather | solution.py:122
  8.7 211.8 %all-gather.14.cloned.1.call-start = ((), (), s32[]{:S(2)}) async-start(), calls=%async_computation.2 | async-start | bytes 2228224 | tf_op jit(solution)/shard_map/all_gather | solution.py:121
  9.3 257.2 %all-gather.18.cloned.1.call-start = ((), (), s32[]{:S(2)}) async-start(), calls=%async_computation.4 | async-start | bytes 2621440 | tf_op jit(solution)/shard_map/all_gather | solution.py:60
  24.3 69.5 %copy-start.9 = (f32[64]{0:T(128)S(1)}, f32[64]{0:T(128)}, u32[]{:S(2)}) copy-start(f32[64]{0:T(128)} %param.23) | copy-start | bytes 772
  24.3 124.3 %copy-start.1 = (bf16[1,512,2048]{2,1,0:T(8,128)(2,1)S(1)}, bf16[1,512,2048]{2,1,0:T(8,128)(2,1)}, u32[]{:S(2)}) copy-start(bf16[1,512,2048]{2,1,0:T(8,128)(2,1)} %all-gather.30.cloned.1.call-done) | copy-start | bytes 6291460
  90.9 252.6 %all-gather.24.cloned.1.call-start = ((), (), s32[]{:S(2)}) async-start(), calls=%async_computation.7 | async-start | bytes 4456448 | tf_op jit(solution)/shard_map/all_gather | solution.py:125
  91.5 329.0 %all-gather.26.cloned.1.call-start = ((), (), s32[]{:S(2)}) async-start(), calls=%async_computation.8 | async-start | bytes 4456448 | tf_op jit(solution)/shard_map/all_gather | solution.py:126
  92.2 405.3 %all-gather.22.cloned.1.call-start = ((), (), s32[]{:S(2)}) async-start(), calls=%async_computation.6 | async-start | bytes 4456448 | tf_op jit(solution)/shard_map/all_gather | solution.py:124
  93.0 481.5 %all-gather.28.cloned.1.call-start = ((), (), s32[]{:S(2)}) async-start(), calls=%async_computation.9 | async-start | bytes 4456448 | tf_op jit(solution)/shard_map/all_gather | solution.py:128
  93.7 542.4 %all-gather.20.cloned.1.call-start = ((), (), s32[]{:S(2)}) async-start(), calls=%async_computation.5 | async-start | bytes 2228224 | tf_op jit(solution)/shard_map/all_gather | solution.py:127
  93.9 74.5 %copy-start.11 = (f32[8]{0:T(128)S(1)}, f32[8]{0:T(128)}, u32[]{:S(2)}) copy-start(f32[8]{0:T(128)} %param.24) | copy-start | bytes 100
  151.8 16.5 %collective-permute-start = (bf16[512,512]{0,1:T(8,128)(2,1)S(1)}, bf16[512,512]{0,1:T(8,128)(2,1)S(1)}, u32[]{:S(2)}, u32[]{:S(2)}) collective-permute-start(bf16[512,512]{0,1:T(8,128)(2,1)S(1)} %fusion.29), channel_id=1, source_target_pairs={{0,8},{8,16},{16,24},{24,0},{1,9},{9,17},{17,25},{25,1},{2,10},{10... | collective-permute-start | bytes 1572872 | tf_op jit(solution)/shard_map/ppermute | solution.py:56
  168.2 56.0 %copy-start.3 = (bf16[512,512]{0,1:T(8,128)(2,1)}, bf16[512,512]{0,1:T(8,128)(2,1)S(1)}, u32[]{:S(2)}) copy-start(bf16[512,512]{0,1:T(8,128)(2,1)S(1)} %collective-permute-done) | copy-start | bytes 1572868
  168.3 13.4 %collective-permute-start.1 = (bf16[512,512]{0,1:T(8,128)(2,1)S(1)}, bf16[512,512]{0,1:T(8,128)(2,1)}, u32[]{:S(2)}, u32[]{:S(2)}) collective-permute-start(bf16[512,512]{0,1:T(8,128)(2,1)S(1)} %collective-permute-done), channel_id=1, source_target_pairs={{0,8},{8,16},{16,24},{24,0},{1,9},{9,17},{17,25},{25,1},{2,10},{10... | collective-permute-start | bytes 1572872 | tf_op jit(solution)/shard_map/ppermute | solution.py:56
  168.3 482.1 %reduce-scatter.2.cloned.1.call-start = ((), (), s32[]{:S(2)}) async-start(), calls=%async_computation.10 | async-start | bytes 3145728 | tf_op jit(solution)/shard_map/reduce_scatter | solution.py:144
  169.4 54.9 %copy-start.7 = (f32[64]{0:T(128)S(1)}, f32[64]{0:T(128)}, u32[]{:S(2)}) copy-start(f32[64]{0:T(128)} %param.22) | copy-start | bytes 772
  181.6 42.9 %collective-permute-start.2 = (bf16[512,512]{0,1:T(8,128)(2,1)}, bf16[512,512]{0,1:T(8,128)(2,1)}, u32[]{:S(2)}, u32[]{:S(2)}) collective-permute-start(bf16[512,512]{0,1:T(8,128)(2,1)} %collective-permute-done.1), channel_id=1, source_target_pairs={{0,8},{8,16},{16,24},{24,0},{1,9},{9,17},{17,25},{25,1},{2,10},{10... | collective-permute-start | bytes 1572872 | tf_op jit(solution)/shard_map/ppermute | solution.py:56
  224.2 2.5 copy-start.4
  276.1 6.3 copy-start
  291.0 6.3 copy-start
  305.7 6.3 copy-start
  320.7 6.3 copy-start
  331.6 2.2 copy-start.8
  333.5 10.0 %copy-start.2 = (bf16[1,512,2048]{2,1,0:T(8,128)(2,1)S(1)}, bf16[1,512,2048]{2,1,0:T(8,128)(2,1)}, u32[]{:S(2)}) copy-start(bf16[1,512,2048]{2,1,0:T(8,128)(2,1)} %all-gather.30.cloned.1.call-done) | copy-start | bytes 6291460
  425.8 1.0 copy-start.5
  426.8 76.5 %collective-permute-start.3 = (bf16[1,1024]{1,0:T(2,128)(2,1)S(1)}, bf16[1,1024]{1,0:T(2,128)(2,1)S(1)}, u32[]{:S(2)}, u32[]{:S(2)}) collective-permute-start(bf16[1,1024]{1,0:T(2,128)(2,1)S(1)} %get-tuple-element.101), channel_id=1, source_target_pairs={{0,8},{8,16},{16,24},{1,9},{9,17},{17,25},{2,10},{10,18},{18,26},{... | collective-permute-start | bytes 6152 | tf_op jit(solution)/shard_map/ppermute | solution.py:17
  430.2 73.1 %collective-permute-start.4 = (bf16[1,1024]{1,0:T(2,128)(2,1)S(1)}, bf16[1,1024]{1,0:T(2,128)(2,1)S(1)}, u32[]{:S(2)}, u32[]{:S(2)}) collective-permute-start(bf16[1,1024]{1,0:T(2,128)(2,1)S(1)} %get-tuple-element.102), channel_id=1, source_target_pairs={{8,0},{16,8},{24,16},{9,1},{17,9},{25,17},{10,2},{18,10},{26,18},{... | collective-permute-start | bytes 6152 | tf_op jit(solution)/shard_map/ppermute | solution.py:18
  497.5 5.7 copy-start.6
Sparse Core Ops, SparseCore 0:
  8.9 13.2 all-gather.29
  25.0 61.5 all-gather.15
  89.3 59.1 all-gather.11
  151.2 69.3 all-gather.13
  222.0 44.4 all-gather.17
  269.1 74.3 all-gather.23
  346.3 74.1 all-gather.25
  423.3 74.1 all-gather.21
  500.3 74.1 all-gather.27
  577.1 58.9 all-gather.19
  641.8 8.5 reduce-scatter.1
